TPU v7x, 32 devices: a whole 2x2x4 slice. The times are simulated.
32 devices in a mesh: kv: 8 (over z, x), tp: 4 (over y, core).
Axes of the slice: x: 2, y: 2, z: 4, core: 2. Of those that a mesh axis runs over, the one named last changes fastest.
Arguments:
- tokens: bfloat16 [22, 4096], P(None, ('kv', 'tp')), may hold values from -22 to 22
- attn_gain: float32 [4096], P('kv'), may hold values from 0.1 to 1.9
- w_query: bfloat16 [4096, 4096], P('kv', 'tp'), may hold values from -0.09375 to 0.09375
- w_key: bfloat16 [4096, 4096], P('kv', 'tp'), may hold values from -0.5 to 0.5
- w_value: bfloat16 [4096, 4096], P('kv', 'tp'), may hold values from -0.09375 to 0.09375
- cache_keys: bfloat16 [22, 2048, 32, 128], P(None, 'kv', 'tp'), may hold values from -256 to 256
- cache_values: bfloat16 [22, 2048, 32, 128], P(None, 'kv', 'tp'), may hold values from -6 to 6
- lambdas: float32 [32], P('tp'), may hold values from 0.3 to 0.8
- head_gain: float32 [128], replicated, may hold values from 0.1 to 1.9
- w_out: bfloat16 [4096, 4096], P('tp', 'kv'), may hold values from -0.09375 to 0.09375
- mlp_gain: float32 [4096], P('kv'), may hold values from 0.1 to 1.9
- w_gate: bfloat16 [4096, 11008], P('kv', 'tp'), may hold values from -0.09375 to 0.09375
- w_up: bfloat16 [4096, 11008], P('kv', 'tp'), may hold values from -0.09375 to 0.09375
- w_down: bfloat16 [11008, 4096], P('tp', 'kv'), may hold values from -0.0546875 to 0.0546875
Outputs:
- output: bfloat16 [22, 4096], P(None, ('kv', 'tp'))
All inputs are finite; a program needn't handle non-finite values.
Results may differ from a plain program's by a relative error of at most 0.017.
The roundings to bfloat16 on the way count: a program that leaves them out, or rounds other values in their place, can miss the bound.
Values may be sent and summed in bfloat16 or wider, within the bound.
A program may use at most 128 MiB of HBM per device.

v0:
```python
import functools

import jax
import jax.numpy as jnp
from jax import lax
from jax.experimental import pallas as pl
from jax.experimental.pallas import tpu as pltpu
from jax.sharding import PartitionSpec as P

epsilon = 1e-06
MESH = pl.DeviceIdType.MESH
F32 = jnp.float32
BF16 = jnp.bfloat16
Q_LINK = jnp.bfloat16
KV_LINK = jnp.float32
FF_LINK = jnp.bfloat16


def partner(me, step, count):
    if count & (count - 1):
        return lax.rem(me + step, count)
    peer, bit = 0, 1
    while bit < count:
        digit = lax.rem(lax.div(me, bit), 2)
        peer = peer + bit * (1 - digit if step & bit else digit)
        bit *= 2
    return peer


def sender(me, step, count):
    if count & (count - 1):
        return lax.rem(me + count - step, count)
    return partner(me, step, count)


def peers(axis, count):
    me = lax.axis_index(axis)
    return [(step, partner(me, step, count)) for step in reversed(range(1, count))]


def exchange(axis, count, source, target, send_sem, recv_sem):
    copies = []
    for step, peer in peers(axis, count):
        copy = pltpu.make_async_remote_copy(
            src_ref=source(peer),
            dst_ref=target,
            send_sem=send_sem.at[step - 1],
            recv_sem=recv_sem.at[step - 1],
            device_id={axis: peer},
            device_id_type=MESH,
        )
        copy.start()
        copies.append(copy)
    return copies


def to_row(column):
    rows = column.shape[0]
    spot = lax.broadcasted_iota(jnp.int32, (rows, 128), 0) == lax.broadcasted_iota(
        jnp.int32, (rows, 128), 1
    )
    return jnp.sum(jnp.where(spot, column, 0.0), axis=0, keepdims=True)


def to_column(row, rows):
    spot = lax.broadcasted_iota(jnp.int32, (rows, 128), 0) == lax.broadcasted_iota(
        jnp.int32, (rows, 128), 1
    )
    return jnp.sum(jnp.where(spot, row, 0.0), axis=1, keepdims=True)


def wait_recv(copies):
    for copy in copies:
        copy.wait_recv()


def wait_send(copies):
    for copy in copies:
        copy.wait_send()


def pad_rows(value, rows):
    if value.shape[0] == rows:
        return value
    return jnp.concatenate(
        [value, jnp.zeros((rows - value.shape[0],) + value.shape[1:], value.dtype)], axis=0
    )


def pad_cols(value, cols):
    if value.shape[1] == cols:
        return value
    return jnp.concatenate(
        [value, jnp.zeros((value.shape[0], cols - value.shape[1]), value.dtype)], axis=1
    )


def layer_kernel(
    dims, tok_in, gain_in, wq_in, wk_in, wv_in, keys_in, values_in, lam_in, head_gain_in, w_out_in,
    mid_gain_in, w_gate_in, w_up_in, w_down_in,
    out,
    tok, gain, lam, head_gain, mid_gain, wq, wk, wv, keys, values, wo, wg, wu, wd,
    tok_all, sq_all, q_part, q_got, q_own, q_all, kv_part, kv_got, q_seq, scores, acc, lse,
    o_in, o_all, l_in, l_all, h_own, h_all, b_all, mid_all, gu_part, gu_all, hid_own, hid_all,
    d_part, d_all,
    w_sem, k_sem, v_sem, *sems,
):
    n_kv, n_tp, groups, rows, width, chunk, per_step = dims
    seqs, own = out.shape
    heads = n_kv // groups
    hubs, first = n_kv // 2, n_kv // 4
    hd = head_gain.shape[1]
    half_dim = hd // 2
    score_scale = half_dim ** (-0.5)
    length = keys.shape[1]
    steps = seqs // per_step
    pairs = [(sems[2 * at], sems[2 * at + 1]) for at in range(len(sems) // 2)]
    t_sem, b_sem, d_sem = pairs[:3]
    sq_sem, m_sem, q_sem, kv_sem, o_sem, l_sem, g_sem = pairs[3:10]
    qa_sem, h_sem, i_sem = pairs[10:13]

    def load(index, source, target):
        copy = pltpu.make_async_copy(source, target, w_sem.at[index])
        copy.start()
        return copy

    load_tok = load(0, tok_in, tok)
    load_gain = load(1, gain_in, gain)
    load_q = load(2, wq_in, wq)
    load_k = load(3, wk_in, wk)
    load_v = load(4, wv_in, wv)

    def cache_copies(step):
        at = pl.ds(step * per_step, per_step)
        return (
            pltpu.make_async_copy(keys_in.at[at], keys.at[at], k_sem.at[step]),
            pltpu.make_async_copy(values_in.at[at], values.at[at], v_sem.at[step]),
        )

    for step in range(steps):
        for copy in cache_copies(step):
            copy.start()
    load_lam = load(5, lam_in, lam)
    load_hg = load(6, head_gain_in, head_gain)
    load_mg = load(7, mid_gain_in, mid_gain)
    load_wo = load(8, w_out_in, wo)
    units = w_down_in.shape[0]
    load_wg = load(9, w_gate_in, wg.at[pl.ds(0, units)])
    load_wu = load(10, w_up_in, wu.at[pl.ds(0, units)])
    load_wd = load(11, w_down_in, wd.at[pl.ds(0, units)])
    if units < hubs * chunk:
        for buf in (wg, wu, wd):
            buf[units:, :] = jnp.zeros((hubs * chunk - units, buf.shape[1]), BF16)

    me = lax.axis_index("kv")
    me_tp = lax.axis_index("tp")
    side = lax.rem(me_tp, 2)
    lead = me_tp + 1 - side
    spot = me - first
    low = 1 - lax.div(me, hubs)
    is_hub = (side == 1) & (me >= first) & (me < first + hubs)
    far_first = [s + low * (hubs - 1 - 2 * s) for s in range(hubs)]
    sent = []

    def hub_at(hub):
        return {"kv": first + hub, "tp": lead}

    def at_home(hub):
        return (side == 1) & (first + hub == me)

    barrier = pltpu.get_barrier_semaphore()

    def greet(device):
        pl.semaphore_signal(barrier, inc=1, device_id=device, device_id_type=MESH)

    for _, peer in peers("tp", n_tp):
        greet({"kv": me, "tp": peer})
    for hub in far_first:
        pl.when(jnp.logical_not(at_home(hub)))(functools.partial(greet, hub_at(hub)))

    @pl.when(is_hub)
    def _():
        for step in reversed(range(n_kv)):
            for part in range(2):
                if step > 0 or part == 0:
                    greet({"kv": partner(me, step, n_kv), "tp": me_tp - 1 + part})
        pl.semaphore_wait(barrier, n_tp - 1 + 2 * n_kv - 1 + hubs - 1)

    @pl.when(jnp.logical_not(is_hub))
    def _():
        pl.semaphore_wait(barrier, n_tp - 1 + hubs)

    def to_hub(hub, s, source, target, sem):
        home = at_home(hub)
        copy = pltpu.make_async_remote_copy(
            src_ref=source,
            dst_ref=target.at[side, me],
            send_sem=sem[0].at[s],
            recv_sem=sem[1].at[side, me],
            device_id=hub_at(hub),
            device_id_type=MESH,
        )
        away = jnp.logical_not(home)
        pl.when(away)(copy.start)

        @pl.when(home)
        def _():
            target[1, me] = source[...]

        sent.append((away, copy))

    def to_hubs(source, target, sem):
        for s, hub in enumerate(far_first):
            to_hub(hub, s, source.at[hub], target, sem)

    def collected(target, sem, part):
        for step in range(part, n_kv):
            peer = sender(me, step, n_kv)
            pltpu.make_async_remote_copy(
                src_ref=target.at[part, peer],
                dst_ref=target.at[part, peer],
                send_sem=sem[0].at[0],
                recv_sem=sem[1].at[part, peer],
                device_id=hub_at(0),
                device_id_type=MESH,
            ).wait_recv()

    def row_copy(hub, s, target, sem):
        return pltpu.make_async_remote_copy(
            src_ref=target.at[me],
            dst_ref=target.at[me],
            send_sem=sem[0].at[s],
            recv_sem=sem[1].at[me],
            device_id=hub_at(hub),
            device_id_type=MESH,
        )

    def rows_to_hubs(target, sem):
        for s, hub in enumerate(far_first):
            away = (side == 1) & jnp.logical_not(at_home(hub))
            copy = row_copy(hub, s, target, sem)
            pl.when(away)(copy.start)
            sent.append((away, copy))

    def row_sum(target, sem):
        for step in range(1, n_kv):
            peer = sender(me, step, n_kv)
            pltpu.make_async_remote_copy(
                src_ref=target.at[peer],
                dst_ref=target.at[peer],
                send_sem=sem[0].at[0],
                recv_sem=sem[1].at[peer],
                device_id=hub_at(0),
                device_id_type=MESH,
            ).wait_recv()
        total = target[0]
        for index in range(1, n_kv):
            total = total + target[index]
        return lax.rsqrt(to_column(total, seqs) / width + epsilon)

    def spread_copy(part, step, source, target, sem):
        return pltpu.make_async_remote_copy(
            src_ref=source.at[part],
            dst_ref=target.at[spot],
            send_sem=sem[0].at[part, step],
            recv_sem=sem[1].at[spot],
            device_id={"kv": partner(me, step, n_kv), "tp": me_tp - 1 + part},
            device_id_type=MESH,
        )

    def spread(part, source, target, sem):
        for step in reversed(range(part, n_kv)):
            spread_copy(part, step, source, target, sem).start()
        if part == 1:
            target[spot] = source[1]

    def arrived(hub, target, sem):
        copy = pltpu.make_async_remote_copy(
            src_ref=target.at[hub],
            dst_ref=target.at[hub],
            send_sem=sem[0].at[0, 0],
            recv_sem=sem[1].at[hub],
            device_id=hub_at(0),
            device_id_type=MESH,
        )
        pl.when(jnp.logical_not(at_home(hub)))(copy.wait_recv)

    load_tok.wait()
    tok_copies = exchange("tp", n_tp, lambda peer: tok, tok_all.at[me_tp], *t_sem)
    tok_all[me_tp] = tok[...]
    load_gain.wait()
    wait_recv(tok_copies)
    xf = jnp.concatenate([tok_all[index] for index in range(n_tp)], axis=1).astype(F32)
    normed = (xf * gain[...]).astype(BF16)

    def project(buf, link):
        product = jnp.dot(normed, buf[...], preferred_element_type=F32).astype(link)
        product = pad_rows(product, groups * rows)
        return [
            product[group * rows : (group + 1) * rows, head * hd : (head + 1) * hd]
            for head in range(heads)
            for group in range(groups)
        ]

    def piece_rows(column, index):
        if groups == 1:
            return column
        column = pad_rows(column, groups * rows)
        group_of = lax.rem(2 * spot + index, groups)
        mine = column[:rows]
        for group in range(1, groups):
            mine = jnp.where(group_of == group, column[group * rows : (group + 1) * rows], mine)
        return mine

    load_q.wait()
    for piece, value in enumerate(project(wq, Q_LINK)):
        q_part[piece // 2, piece % 2] = value
    to_hubs(q_part, q_got, q_sem)
    sq_all[me] = to_row(jnp.sum(xf * xf, axis=1, keepdims=True))
    rows_to_hubs(sq_all, sq_sem)
    load_k.wait()
    for piece, value in enumerate(project(wk, KV_LINK)):
        kv_part[piece // 2, piece % 2, 0] = value
    load_v.wait()
    for piece, value in enumerate(project(wv, KV_LINK)):
        kv_part[piece // 2, piece % 2, 1] = value

    @pl.when(is_hub)
    def _():
        scale = row_sum(sq_all, sq_sem)
        for part in (1, 0):
            collected(q_got, q_sem, part)
            for index in range(2):
                total = q_got[part, 0, index].astype(F32)
                for source in range(1, n_kv):
                    total = total + q_got[part, source, index].astype(F32)
                q_own[part, index] = (piece_rows(scale, index) * total).astype(BF16)
            spread(part, q_own, q_all, qa_sem)

    for hub in range(hubs):
        arrived(hub, q_all, qa_sem)
    to_hubs(kv_part, kv_got, kv_sem)
    for piece in range(n_kv):
        head, group = piece // groups, piece % groups
        q_seq[group * rows : (group + 1) * rows, head : head + 1, :] = q_all[
            piece // 2, piece % 2
        ].astype(F32)[:, None, :]

    row = lax.broadcasted_iota(jnp.int32, (2 * heads * per_step, length), 0)
    col = lax.broadcasted_iota(jnp.int32, (2 * heads * per_step, length), 1)
    keep = lax.rem(col, heads) == lax.rem(row, heads)
    stat_lane = lax.broadcasted_iota(jnp.int32, (2 * heads, 128), 1)
    q_lane = lax.broadcasted_iota(jnp.int32, (heads, hd), 1)
    lse[...] = jnp.zeros_like(lse)

    def queries(seq):
        vec = q_seq[seq]
        return jnp.concatenate(
            [jnp.where(q_lane < half_dim, vec, 0.0), jnp.where(q_lane < half_dim, 0.0, vec)],
            axis=0,
        ).astype(BF16)

    def wide(parts):
        return parts[0] if per_step == 1 else jnp.concatenate(parts, axis=1)

    def score(at):
        span = range(at * per_step, (at + 1) * per_step)
        blank = jnp.zeros((2 * heads, hd), BF16)
        query = jnp.concatenate(
            [wide([queries(seq) if other == seq else blank for other in span]) for seq in span],
            axis=0,
        )
        scores[at % 2] = lax.dot_general(
            query, wide([keys[seq] for seq in span]), (((1,), (1,)), ((), ())),
            preferred_element_type=F32,
        )

    def attend(at):
        span = range(at * per_step, (at + 1) * per_step)
        level = jnp.where(keep, scores[at % 2] * score_scale, -jnp.inf)
        peak = jnp.max(level, axis=1, keepdims=True)
        weights = jnp.exp(level - peak)
        total = jnp.sum(weights, axis=1, keepdims=True)
        summed = jnp.dot(
            weights.astype(BF16), wide([values[seq] for seq in span]), preferred_element_type=F32
        )
        result = summed / total
        level = peak + jnp.log(total)
        stats = lse[...]
        for index, seq in enumerate(span):
            part = slice(index * 2 * heads, (index + 1) * 2 * heads)
            acc[:, seq : seq + 1, :] = result[part, index * hd : (index + 1) * hd][:, None, :]
            stats = jnp.where(stat_lane == seq, level[part], stats)
        lse[...] = stats

    for step in range(steps):
        for copy in cache_copies(step):
            copy.wait()
    score(0)
    for step in range(steps):
        if step + 1 < steps:
            score(step + 1)
        attend(step)

    load_lam.wait()
    last_lane = lax.broadcasted_iota(jnp.int32, (1, 128), 1) == 127
    for piece in range(n_kv):
        head, group = piece // groups, piece % groups
        span = slice(group * rows, (group + 1) * rows)
        for half in range(2):
            at = half * heads + head
            o_in[piece // 2, piece % 2, half] = acc[at, span, :].astype(BF16)
            l_in[piece // 2, 2 * (piece % 2) + half : 2 * (piece % 2) + half + 1, :] = jnp.where(
                last_lane, lam[:, head : head + 1], pad_cols(lse[at : at + 1, span], 128)
            )
    to_hubs(l_in, l_all, l_sem)
    to_hubs(o_in, o_all, o_sem)
    load_hg.wait()
    load_mg.wait()

    @pl.when(is_hub)
    def _():
        total = sq_all[0]
        for index in range(1, n_kv):
            total = total + sq_all[index]
        scale = lax.rsqrt(to_column(total, seqs) / width + epsilon)
        lane = lax.broadcasted_iota(jnp.int32, (rows, hd), 1)
        fresh, value_new = {}, {}
        for part in (1, 0):
            collected(kv_got, kv_sem, part)
            for index in range(2):
                mine = piece_rows(scale, index)
                k_sum, v_sum = kv_got[part, 0, index, 0], kv_got[part, 0, index, 1]
                for source in range(1, n_kv):
                    k_sum = k_sum + kv_got[part, source, index, 0]
                    v_sum = v_sum + kv_got[part, source, index, 1]
                k_new = (mine * k_sum).astype(BF16).astype(F32)
                value_new[part, index] = (mine * v_sum).astype(BF16).astype(F32)
                product = q_own[part, index].astype(F32) * k_new
                for half in range(2):
                    inside = (lane < half_dim) if half == 0 else (lane >= half_dim)
                    fresh[part, index, half] = to_row(
                        jnp.sum(jnp.where(inside, product, 0.0), axis=1, keepdims=True)
                        * score_scale
                    )
        for part in (1, 0):
            collected(l_all, l_sem, part)
            shares = []
            for index in range(2):
                for half in range(2):
                    at = 2 * index + half
                    level = jnp.concatenate(
                        [l_all[part, source, at : at + 1, :] for source in range(n_kv)]
                        + [fresh[part, index, half]],
                        axis=0,
                    )
                    share = jnp.exp(level - jnp.max(level, axis=0, keepdims=True))
                    share = share / jnp.sum(share, axis=0, keepdims=True)
                    if half == 1:
                        share = share * -l_all[part, 0, at : at + 1, 127:]
                    shares.append(share)
            count = n_kv + 1
            columns = []
            for begin in range(0, 4, max(1, 128 // count)):
                block = jnp.concatenate(shares[begin : begin + max(1, 128 // count)], axis=0)
                turned = jnp.transpose(pad_rows(block, 128))
                columns += [
                    turned[:rows, at : at + 1] for at in range(block.shape[0])
                ]
            collected(o_all, o_sem, part)
            for index in range(2):
                difference = 0.0
                for half in range(2):
                    at = (2 * index + half) * count
                    top = columns[at + n_kv] * value_new[part, index]
                    for source in range(n_kv):
                        top = top + columns[at + source] * o_all[part, source, index, half].astype(
                            F32
                        )
                    difference = difference + top
                normal = (
                    difference
                    * lax.rsqrt(jnp.mean(difference * difference, axis=1, keepdims=True) + epsilon)
                    * head_gain[...]
                )
                h_own[part, index] = normal.astype(BF16)
            spread(part, h_own, h_all, h_sem)

    load_wo.wait()
    if groups == 1:
        shared = None
        for hub in reversed(far_first):
            arrived(hub, h_all, h_sem)
            share = jnp.dot(
                jnp.concatenate([h_all[hub, 0], h_all[hub, 1]], axis=1),
                wo[pl.ds(pl.multiple_of(hub * 2 * hd, 2 * hd), 2 * hd), :],
                preferred_element_type=F32,
            )
            shared = share if shared is None else shared + share
    else:
        for hub in range(hubs):
            arrived(hub, h_all, h_sem)
        columns = []
        for head in range(heads):
            pieces = range(head * groups, (head + 1) * groups)
            column = [h_all[piece // 2, piece % 2].astype(F32) for piece in pieces]
            columns.append(jnp.concatenate(column, axis=0)[:seqs].astype(BF16))
        shared = jnp.dot(
            jnp.concatenate(columns, axis=1), wo[...], preferred_element_type=F32
        )
    b_all[me_tp] = shared.astype(BF16)
    b_copies = exchange("tp", n_tp, lambda peer: b_all.at[me_tp], b_all.at[me_tp], *b_sem)
    wait_recv(b_copies)
    branch = b_all[0].astype(F32)
    for index in range(1, n_tp):
        branch = branch + b_all[index].astype(F32)
    residual = (xf + branch).astype(BF16)
    res_f = residual.astype(F32)
    normed_mid = (res_f * mid_gain[...]).astype(BF16)
    load_wg.wait()
    load_wu.wait()
    for s, hub in enumerate(far_first):
        at = pl.ds(pl.multiple_of(hub * chunk, 16), chunk)
        gu_part[s] = lax.dot_general(
            normed_mid, jnp.concatenate([wg[at, :], wu[at, :]], axis=0),
            (((1,), (1,)), ((), ())), preferred_element_type=F32,
        ).astype(FF_LINK)
        to_hub(hub, s, gu_part.at[s], gu_all, g_sem)
        if s == 0:
            mid_all[me] = to_row(jnp.sum(res_f * res_f, axis=1, keepdims=True))
            rows_to_hubs(mid_all, m_sem)

    @pl.when(is_hub)
    def _():
        scale = row_sum(mid_all, m_sem)
        for part in (1, 0):
            collected(gu_all, g_sem, part)
            total = gu_all[part, 0].astype(F32)
            for source in range(1, n_kv):
                total = total + gu_all[part, source].astype(F32)
            gate, up = scale * total[:, :chunk], scale * total[:, chunk:]
            hid_own[part] = (gate / (1.0 + jnp.exp(-gate)) * up).astype(BF16)
            spread(part, hid_own, hid_all, i_sem)

    load_wd.wait()
    down = None
    for hub in reversed(far_first):
        arrived(hub, hid_all, i_sem)
        share = jnp.dot(
            hid_all[hub],
            wd[pl.ds(pl.multiple_of(hub * chunk, 16), chunk), :],
            preferred_element_type=F32,
        )
        down = share if down is None else down + share
    down = down.astype(BF16)
    for index in range(n_tp):
        d_part[index] = down[:, index * own : (index + 1) * own]
    d_copies = exchange("tp", n_tp, lambda peer: d_part.at[peer], d_all.at[me_tp], *d_sem)
    d_all[me_tp] = d_part[me_tp]
    base = res_f[:, :own]
    for index in range(1, n_tp):
        base = jnp.where(me_tp == index, res_f[:, index * own : (index + 1) * own], base)
    wait_recv(d_copies)
    mixer = d_all[0].astype(F32)
    for index in range(1, n_tp):
        mixer = mixer + d_all[index].astype(F32)
    out[...] = (base + mixer).astype(BF16)
    wait_send(tok_copies + b_copies + d_copies)
    for away, copy in sent:
        pl.when(away)(copy.wait_send)

    @pl.when(is_hub)
    def _():
        for source, target, sem in (
            (q_own, q_all, qa_sem), (h_own, h_all, h_sem), (hid_own, hid_all, i_sem)
        ):
            for part in range(2):
                for step in range(part, n_kv):
                    spread_copy(part, step, source, target, sem).wait_send()


ANY = pl.BlockSpec(memory_space=pl.ANY)


def per_device(
    n_kv, n_tp, tokens, attn_gain, w_query, w_key, w_value, cache_keys, cache_values, lambdas,
    head_gain, w_out, mlp_gain, w_gate, w_up, w_down,
):
    seqs, own = tokens.shape
    heads = lambdas.shape[0]
    hd = head_gain.shape[0]
    feats = attn_gain.shape[0]
    width = feats * n_kv
    groups = n_kv // heads
    rows = -(-seqs // groups)
    units = w_gate.shape[1]
    hubs = n_kv // 2
    chunk = 16 * -(-units // (16 * hubs))
    length = cache_keys.shape[1] * heads
    per_step = 2 if seqs % 2 == 0 else 1
    dma = pltpu.SemaphoreType.DMA
    tp_sems = [dma((n_tp - 1,)), dma((n_tp - 1,))]
    row_sems = [dma((hubs,)), dma((n_kv,))]
    hub_sems = [dma((hubs,)), dma((2, n_kv))]
    out_sems = [dma((2, n_kv)), dma((hubs,))]
    vm = pltpu.VMEM
    return pl.pallas_call(
        functools.partial(layer_kernel, (n_kv, n_tp, groups, rows, width, chunk, per_step)),
        out_shape=pltpu.VMEM((seqs, own), BF16),
        in_specs=[ANY] * 14,
        out_specs=pl.BlockSpec(memory_space=pltpu.VMEM),
        scratch_shapes=[
            vm((seqs, own), BF16),
            vm((1, feats), F32),
            vm((1, heads), F32),
            vm((1, hd), F32),
            vm((1, feats), F32),
            vm(w_query.shape, BF16),
            vm(w_key.shape, BF16),
            vm(w_value.shape, BF16),
            vm((seqs, length, hd), BF16),
            vm((seqs, length, hd), BF16),
            vm(w_out.shape, BF16),
            vm((hubs * chunk, feats), BF16),
            vm((hubs * chunk, feats), BF16),
            vm((hubs * chunk, w_down.shape[1]), BF16),
            vm((n_tp, seqs, own), BF16),
            vm((n_kv, 1, 128), F32),
            vm((hubs, 2, rows, hd), Q_LINK),
            vm((2, n_kv, 2, rows, hd), Q_LINK),
            vm((2, 2, rows, hd), BF16),
            vm((hubs, 2, rows, hd), BF16),
            vm((hubs, 2, 2, rows, hd), KV_LINK),
            vm((2, n_kv, 2, 2, rows, hd), KV_LINK),
            vm((groups * rows, heads, hd), F32),
            vm((2, 2 * heads * per_step, length), F32),
            vm((2 * heads, groups * rows, hd), F32),
            vm((2 * heads, 128), F32),
            vm((hubs, 2, 2, rows, hd), BF16),
            vm((2, n_kv, 2, 2, rows, hd), BF16),
            vm((hubs, 4, 128), F32),
            vm((2, n_kv, 4, 128), F32),
            vm((2, 2, rows, hd), BF16),
            vm((hubs, 2, rows, hd), BF16),
            vm((n_tp, seqs, feats), BF16),
            vm((n_kv, 1, 128), F32),
            vm((hubs, seqs, 2 * chunk), FF_LINK),
            vm((2, n_kv, seqs, 2 * chunk), FF_LINK),
            vm((2, seqs, chunk), BF16),
            vm((hubs, seqs, chunk), BF16),
            vm((n_tp, seqs, own), BF16),
            vm((n_tp, seqs, own), BF16),
            dma((12,)), dma((seqs // per_step,)), dma((seqs // per_step,)),
            *(tp_sems * 3), *(row_sems * 2), *(hub_sems * 5), *(out_sems * 3),
        ],
        compiler_params=pltpu.CompilerParams(
            collective_id=0, has_side_effects=True, vmem_limit_bytes=62 << 20
        ),
        name="layer",
    )(
        tokens, attn_gain.reshape(1, feats), w_query, w_key, w_value,
        cache_keys.reshape(seqs, length, hd), cache_values.reshape(seqs, length, hd),
        lambdas.reshape(1, heads), head_gain.reshape(1, hd), w_out, mlp_gain.reshape(1, feats),
        w_gate.T, w_up.T, w_down,
    )


def solution(mesh):
    in_specs = (
        P(None, ("kv", "tp")), P("kv"), P("kv", "tp"), P("kv", "tp"), P("kv", "tp"),
        P(None, "kv", "tp", None), P(None, "kv", "tp", None), P("tp"), P(),
        P("tp", "kv"), P("kv"), P("kv", "tp"), P("kv", "tp"), P("tp", "kv"),
    )
    return jax.shard_map(
        functools.partial(per_device, mesh.shape["kv"], mesh.shape["tp"]),
        mesh=mesh, in_specs=in_specs, out_specs=P(None, ("kv", "tp")), check_vma=False,
    )
```

profile of v0, /device:TPU:0, one launch (start us, length us, event | category | flops | bytes accessed | tf_op | source)
XLA Modules:
  0.0 49.4 jit_solution(10958024903490422862)
XLA Ops:
  0.0 48.8 %layer.1 = bf16[22,128]{1,0:T(8,128)(2,1)S(1)} custom-call(bf16[22,128]{1,0:T(8,128)(2,1)} %tok_in.1, f32[1,512]{1,0:T(1,128)} %bitcast.12, bf16[512,1024]{1,0:T(8,128)(2,1)} %wq_in.1, bf16[512,1024]{1,0:T(8,128)(2,1)} %wk_in.1, bf16[512,1024]{1,0:T(8,128)(2,1)} %wv_in.1, bf16[22,2048,128]{2,1,0:T(8,128)(2,1)} %bitcast.8, bf16[22,2048,128]{2,1,0:T(8,128)(2,1)} %bitcast.9, ...), custom_call_target="tpu_custom_call" | custom-call | tf_op jit(solution)/shard_map/layer/pallas_call | solution.py:607
  48.8 0.6 %copy.16 = bf16[22,128]{1,0:T(8,128)(2,1)} copy(bf16[22,128]{1,0:T(8,128)(2,1)S(1)} %layer.1) | data formatting | bytes 11264
where the time goes:
time: 49.6 us; the launch traced here: 49.4 us
  Pallas kernels  48.8 us (98%)
  local copies, waits for them, and re-layouts  0.6 us (1%)
    pallas_call x1, Pallas kernels, per_device(): pl.pallas_call(functools.partial(layer_kernel, (n_kv, n_tp, groups, rows,...  48.8 us

commit v1 on v0

--- a/solution.py
+++ b/solution.py
@@ -101,7 +101,7 @@
     out,
     tok, gain, lam, head_gain, mid_gain, wq, wk, wv, keys, values, wo, wg, wu, wd,
     tok_all, sq_all, q_part, q_got, q_own, q_all, kv_part, kv_got, q_seq, scores, acc, lse,
-    o_in, o_all, l_in, l_all, h_own, h_all, b_all, mid_all, gu_part, gu_all, hid_own, hid_all,
+    o_in, o_all, l_in, l_all, h_own, h_all, spread_w, b_all, mid_all, gu_part, gu_all, hid_own, hid_all,
     d_part, d_all,
     w_sem, k_sem, v_sem, *sems,
 ):
@@ -190,7 +190,7 @@
     def _():
         pl.semaphore_wait(barrier, n_tp - 1 + hubs)
 
-    def to_hub(hub, s, source, target, sem):
+    def to_hub(hub, s, source, target, sem, late=None):
         home = at_home(hub)
         copy = pltpu.make_async_remote_copy(
             src_ref=source,
@@ -201,7 +201,11 @@
             device_id_type=MESH,
         )
         away = jnp.logical_not(home)
-        pl.when(away)(copy.start)
+        if late is None:
+            pl.when(away)(copy.start)
+        else:
+            pl.when(away & (side != 0))(copy.start)
+            late.append((away & (side == 0), copy))
 
         @pl.when(home)
         def _():
@@ -289,13 +293,32 @@
     tok_copies = exchange("tp", n_tp, lambda peer: tok, tok_all.at[me_tp], *t_sem)
     tok_all[me_tp] = tok[...]
     load_gain.wait()
-    wait_recv(tok_copies)
+    tok_order = [(None, me_tp)] + [
+        (copy, partner(me_tp, n_tp - 1 - at, n_tp)) for at, copy in reversed(list(enumerate(tok_copies)))
+    ]
+    by_part = own % 128 == 0
+    q_product = None
+    if by_part:
+        load_q.wait()
+        for order in range(n_tp):
+            peer = tok_order[order][1]
+            if order > 0:
+                tok_order[order][0].wait_recv()
+            at = pl.ds(pl.multiple_of(peer * own, own), own)
+            share = jnp.dot(
+                (tok_all[peer].astype(F32) * gain[:, at]).astype(BF16), wq[at, :],
+                preferred_element_type=F32,
+            )
+            q_product = share if q_product is None else q_product + share
+    else:
+        wait_recv(tok_copies)
     xf = jnp.concatenate([tok_all[index] for index in range(n_tp)], axis=1).astype(F32)
     normed = (xf * gain[...]).astype(BF16)
 
-    def project(buf, link):
-        product = jnp.dot(normed, buf[...], preferred_element_type=F32).astype(link)
-        product = pad_rows(product, groups * rows)
+    def project(buf, link, product=None):
+        if product is None:
+            product = jnp.dot(normed, buf[...], preferred_element_type=F32)
+        product = pad_rows(product.astype(link), groups * rows)
         return [
             product[group * rows : (group + 1) * rows, head * hd : (head + 1) * hd]
             for head in range(heads)
@@ -312,8 +335,9 @@
             mine = jnp.where(group_of == group, column[group * rows : (group + 1) * rows], mine)
         return mine
 
-    load_q.wait()
-    for piece, value in enumerate(project(wq, Q_LINK)):
+    if not by_part:
+        load_q.wait()
+    for piece, value in enumerate(project(wq, Q_LINK, q_product)):
         q_part[piece // 2, piece % 2] = value
     to_hubs(q_part, q_got, q_sem)
     sq_all[me] = to_row(jnp.sum(xf * xf, axis=1, keepdims=True))
@@ -460,24 +484,35 @@
                         share = share * -l_all[part, 0, at : at + 1, 127:]
                     shares.append(share)
             count = n_kv + 1
-            columns = []
+            at_column = 0
             for begin in range(0, 4, max(1, 128 // count)):
                 block = jnp.concatenate(shares[begin : begin + max(1, 128 // count)], axis=0)
                 turned = jnp.transpose(pad_rows(block, 128))
-                columns += [
-                    turned[:rows, at : at + 1] for at in range(block.shape[0])
-                ]
+                for at in range(block.shape[0]):
+                    spread_w[at_column] = jnp.broadcast_to(turned[:rows, at : at + 1], (rows, hd))
+                    at_column += 1
+            base_value = []
+            for index in range(2):
+                at = 2 * index * count + n_kv
+                base_value.append(
+                    (spread_w[at] + spread_w[at + count]) * value_new[part, index]
+                )
             collected(o_all, o_sem, part)
             for index in range(2):
-                difference = 0.0
+                tops = []
                 for half in range(2):
                     at = (2 * index + half) * count
-                    top = columns[at + n_kv] * value_new[part, index]
-                    for source in range(n_kv):
-                        top = top + columns[at + source] * o_all[part, source, index, half].astype(
-                            F32
-                        )
-                    difference = difference + top
+                    terms = [
+                        spread_w[at + source] * o_all[part, source, index, half].astype(F32)
+                        for source in range(n_kv)
+                    ]
+                    while len(terms) > 1:
+                        terms = [
+                            terms[i] + terms[i + 1] if i + 1 < len(terms) else terms[i]
+                            for i in range(0, len(terms), 2)
+                        ]
+                    tops.append(terms[0])
+                difference = base_value[index] + tops[0] + tops[1]
                 normal = (
                     difference
                     * lax.rsqrt(jnp.mean(difference * difference, axis=1, keepdims=True) + epsilon)
@@ -519,17 +554,20 @@
     normed_mid = (res_f * mid_gain[...]).astype(BF16)
     load_wg.wait()
     load_wu.wait()
+    late = []
     for s, hub in enumerate(far_first):
         at = pl.ds(pl.multiple_of(hub * chunk, 16), chunk)
         gu_part[s] = lax.dot_general(
             normed_mid, jnp.concatenate([wg[at, :], wu[at, :]], axis=0),
             (((1,), (1,)), ((), ())), preferred_element_type=F32,
         ).astype(FF_LINK)
-        to_hub(hub, s, gu_part.at[s], gu_all, g_sem)
+        to_hub(hub, s, gu_part.at[s], gu_all, g_sem, late)
         if s == 0:
             mid_all[me] = to_row(jnp.sum(res_f * res_f, axis=1, keepdims=True))
             rows_to_hubs(mid_all, m_sem)
 
+    for when, copy in late:
+        pl.when(when)(copy.start)
     @pl.when(is_hub)
     def _():
         scale = row_sum(mid_all, m_sem)
@@ -642,6 +680,7 @@
             vm((2, n_kv, 4, 128), F32),
             vm((2, 2, rows, hd), BF16),
             vm((hubs, 2, rows, hd), BF16),
+            vm((4 * (n_kv + 1), rows, hd), F32),
             vm((n_tp, seqs, feats), BF16),
             vm((n_kv, 1, 128), F32),
             vm((hubs, seqs, 2 * chunk), FF_LINK),

time: 49.6 us -> 48.8 us (0.984)
  Pallas kernels: 48.8 us -> 48 us
    pallas_call x1, Pallas kernels: 48.8 us -> 48 us  [per_device(): pl.pallas_call(functools.partial(layer_kernel, (n_kv, n_tp, groups, rows,...]
where the time goes in v1:
time: 48.8 us; the launch traced here: 48.6 us
  Pallas kernels  48 us (98%)
  local copies, waits for them, and re-layouts  0.6 us (1%)
    pallas_call x1, Pallas kernels, per_device(): pl.pallas_call(functools.partial(layer_kernel, (n_kv, n_tp, groups, rows,...  48 us

profile of v1, /device:TPU:0, one launch (start us, length us, event | category | flops | bytes accessed | tf_op | source)
XLA Modules:
  0.0 48.6 jit_solution(10058136011560637835)
XLA Ops:
  0.0 48.0 %layer.1 = bf16[22,128]{1,0:T(8,128)(2,1)S(1)} custom-call(bf16[22,128]{1,0:T(8,128)(2,1)} %tok_in.1, f32[1,512]{1,0:T(1,128)} %bitcast.12, bf16[512,1024]{1,0:T(8,128)(2,1)} %wq_in.1, bf16[512,1024]{1,0:T(8,128)(2,1)} %wk_in.1, bf16[512,1024]{1,0:T(8,128)(2,1)} %wv_in.1, bf16[22,2048,128]{2,1,0:T(8,128)(2,1)} %bitcast.8, bf16[22,2048,128]{2,1,0:T(8,128)(2,1)} %bitcast.9, ...), custom_call_target="tpu_custom_call" | custom-call | tf_op jit(solution)/shard_map/layer/pallas_call | solution.py:645
  48.0 0.6 %copy.16 = bf16[22,128]{1,0:T(8,128)(2,1)} copy(bf16[22,128]{1,0:T(8,128)(2,1)S(1)} %layer.1) | data formatting | bytes 11264
